TPU v7x, 256 devices: a whole 4x4x8 slice. The times are simulated.
256 devices in a mesh: sp: 32 (over z, y), tp: 8 (over x, core).
Axes of the slice: x: 4, y: 4, z: 8, core: 2. Of those that a mesh axis runs over, the one named last changes fastest.
Arguments:
- query_a: bfloat16 [6144, 2048], P('sp', 'tp'), may hold values from -7.5 to 7.5
- key_a: bfloat16 [6144, 1024], P('sp', 'tp'), may hold values from -7.5 to 7.5
- value_a: bfloat16 [6144, 1024], P('sp', 'tp'), may hold values from -6 to 6
- query_b: bfloat16 [6144, 2048], P('sp', 'tp'), may hold values from -7.5 to 7.5
- key_b: bfloat16 [6144, 512], P('sp', 'tp'), may hold values from -7.5 to 7.5
- value_b: bfloat16 [6144, 512], P('sp', 'tp'), may hold values from -6 to 6
- gain_a: float32 [2, 128], replicated, may hold values from 1 to 6.5
- gain_b: float32 [2, 64], replicated, may hold values from 1 to 8.5
- out_a: bfloat16 [2048, 4096], P('tp'), may hold values from -0.5 to 0.5
- out_b: bfloat16 [2048, 4096], P('tp'), may hold values from -0.5 to 0.5
- residual: bfloat16 [6144, 4096], P('sp'), may hold values from -6 to 6
- norm_gain: float32 [4096], replicated, may hold values from 0.1 to 1.9
- gate_weight: bfloat16 [4096, 6144], P('sp', 'tp'), may hold values from -0.09375 to 0.09375
- up_weight: bfloat16 [4096, 6144], P('sp', 'tp'), may hold values from -0.09375 to 0.09375
- down_weight: bfloat16 [6144, 4096], P('tp', 'sp'), may hold values from -0.3125 to 0.3125
Outputs:
- output: bfloat16 [6144, 4096], P(('sp', 'tp'))
All inputs are finite; a program needn't handle non-finite values.
Results may differ from a plain program's by a relative error of at most 0.017.
The roundings to bfloat16 on the way count: a program that leaves them out, or rounds other values in their place, can miss the bound.
Values may be sent and summed in bfloat16 or wider, within the bound.
No kernel may reach another device: no remote copies, remote signals or barrier semaphores. Data moves between devices by JAX's collectives and lax.ppermute only.
A program may use at most 128 MiB of HBM per device.

v0:
```python
import jax
import jax.numpy as jnp
from jax import lax
from jax.sharding import PartitionSpec as P

HEAD_A = 128
HEAD_B = 64
GRID_W = 64
epsilon = 1e-06
theta_base = 10000.0


def rows_first(arrays, axis, dims):
    turned = [jnp.moveaxis(a, dim, 0) for a, dim in zip(arrays, dims)]
    both = jnp.concatenate([t.reshape(len(t), -1) for t in turned], axis=1)
    filled, at, outs = (lax.all_gather(both, axis, axis=0, tiled=True), 0, [])
    for t, dim in zip(turned, dims):
        share = filled[:, at : at + t[0].size].reshape(-1, *t.shape[1:])
        outs.append(jnp.moveaxis(share, 0, dim))
        at += t[0].size
    return tuple(outs)


def side_by_side(arrays, axis, dim, along):
    widths = [a.shape[along] for a in arrays]
    both = jnp.concatenate(arrays, axis=along)
    filled = lax.all_gather(both, axis, axis=dim, tiled=True)
    return tuple(jnp.split(filled, [sum(widths[:k]) for k in range(1, len(widths))], axis=along))


def cut_along(value, dim, devices):
    dims = value.shape
    parts = value.reshape(*dims[:dim], devices, dims[dim] // devices, *dims[dim + 1 :])
    return jnp.moveaxis(parts, dim, 0)


def sum_at_owner(value, axis, dim):
    parts = cut_along(value, dim, lax.axis_size(axis))
    arrived = lax.all_to_all(parts, axis, split_axis=0, concat_axis=0, tiled=True)
    return arrived.astype(jnp.float32).sum(axis=0)


def copy_for_each(value, axis):
    devices = lax.axis_size(axis)
    return lax.all_to_all(
        jnp.broadcast_to(value[None], (devices, *value.shape)), axis, 0, 0, tiled=True
    )


def laid_out(parts, dim):
    dims = list(parts.shape[1:])
    dims[dim] *= parts.shape[0]
    return jnp.moveaxis(parts, 0, dim).reshape(dims)


def gathered_copies(value, axis, dim):
    parts = copy_for_each(value, axis)
    return laid_out(parts, dim)


def rotate(inputs, num_heads, head_size, first_pos, gain):
    tok_rows = inputs.shape[0]
    vectors = inputs.astype(jnp.float32).reshape(tok_rows, num_heads, head_size)
    vectors = (
        vectors * lax.rsqrt(jnp.mean(vectors * vectors, axis=-1, keepdims=True) + epsilon) * gain
    )
    position = first_pos + jnp.arange(tok_rows, dtype=jnp.int32)
    grid_row = (position // GRID_W).astype(jnp.float32)
    grid_col = (position % GRID_W).astype(jnp.float32)
    quarter = head_size // 4
    inv_freq = theta_base ** (-4.0 * jnp.arange(quarter, dtype=jnp.float32) / head_size)
    angle_row = grid_row[:, None] * inv_freq[None, :]
    angle_col = grid_col[:, None] * inv_freq[None, :]
    angles = jnp.concatenate([angle_row, angle_row, angle_col, angle_col], axis=-1)
    quarters = vectors.reshape(tok_rows, num_heads, 4, quarter)
    rotated = jnp.stack(
        [-quarters[:, :, 1], quarters[:, :, 0], -quarters[:, :, 3], quarters[:, :, 2]], axis=2
    )
    rotated = rotated.reshape(tok_rows, num_heads, head_size)
    result = vectors * jnp.cos(angles)[:, None, :] + rotated * jnp.sin(angles)[:, None, :]
    return result.reshape(tok_rows, num_heads * head_size).astype(jnp.bfloat16)


def start_state(kv_heads, groups, tok_rows, head_size):
    return (
        jnp.full((kv_heads, groups, tok_rows), -1e30, jnp.float32),
        jnp.zeros((kv_heads, groups, tok_rows), jnp.float32),
        jnp.zeros((kv_heads, groups, tok_rows, head_size), jnp.float32),
    )


def attend(state, queries, key_rows, values, head_size):
    run_max, run_sum, run_acc = state
    kv_heads = key_rows.shape[1] // head_size
    groups = run_max.shape[1]
    q_heads = queries.reshape(queries.shape[0], kv_heads, groups, head_size)
    k_heads = key_rows.reshape(key_rows.shape[0], kv_heads, head_size)
    v_heads = values.reshape(values.shape[0], kv_heads, head_size)
    scores = jnp.einsum(
        "tkgd,pkd->kgtp", q_heads, k_heads, preferred_element_type=jnp.float32
    ) * head_size ** (-0.5)
    new_max = jnp.maximum(run_max, jnp.max(scores, axis=-1))
    exp_scores = jnp.exp(scores - new_max[..., None])
    new_sum = jnp.sum(exp_scores, axis=-1)
    new_acc = jnp.einsum(
        "kgtp,pkd->kgtd",
        exp_scores.astype(jnp.bfloat16),
        v_heads,
        preferred_element_type=jnp.float32,
    )
    return (new_max, new_sum, new_acc)


def finish(state, num_cols):
    blended = state[2] / state[1][..., None]
    return blended.transpose(2, 0, 1, 3).reshape(blended.shape[2], num_cols).astype(jnp.bfloat16)


def normalize(mixed_rows, gain):
    scale = lax.rsqrt(jnp.mean(mixed_rows * mixed_rows, axis=-1, keepdims=True) + epsilon)
    return (mixed_rows * scale * gain).astype(jnp.bfloat16)


def on_device(
    query_a,
    key_a,
    value_a,
    query_b,
    key_b,
    value_b,
    gain_a,
    gain_b,
    out_a,
    out_b,
    residual,
    norm_gain,
    gate_weight,
    up_weight,
    down_weight,
):
    tok_rows = query_a.shape[0]
    first_pos = lax.axis_index("sp") * tok_rows
    heads_a = query_a.shape[1] // HEAD_A
    heads_b = query_b.shape[1] // HEAD_B
    kv_heads_a = key_a.shape[1] // HEAD_A
    kv_heads_b = key_b.shape[1] // HEAD_B
    kv_width_b = kv_heads_b * HEAD_B
    turned_qa = rotate(query_a, heads_a, HEAD_A, first_pos, gain_a[0])
    turned_ka = rotate(key_a, kv_heads_a, HEAD_A, first_pos, gain_a[1])
    turned_qb = rotate(query_b, heads_b, HEAD_B, first_pos, gain_b[0])
    turned_kb = rotate(key_b, kv_heads_b, HEAD_B, first_pos, gain_b[1])
    pair_b = jnp.concatenate([turned_kb, value_b], axis=1)
    gate_full, up_full, down_full = rows_first(
        (gate_weight, up_weight, down_weight), "sp", (0, 0, 1)
    )
    initial = (
        start_state(kv_heads_a, heads_a // kv_heads_a, tok_rows, HEAD_A),
        start_state(kv_heads_b, heads_b // kv_heads_b, tok_rows, HEAD_B),
    )
    pieces = side_by_side((turned_ka, value_a, pair_b), "sp", 0, 1)
    state_a = attend(initial[0], turned_qa, pieces[0], pieces[1], HEAD_A)
    state_b = attend(
        initial[1], turned_qb, pieces[2][:, :kv_width_b], pieces[2][:, kv_width_b:], HEAD_B
    )
    attn_a = finish(state_a, query_a.shape[1])
    attn_b = finish(state_b, query_b.shape[1])
    own_rows = tok_rows // lax.axis_size("tp")
    own_start = lax.axis_index("tp") * own_rows
    head_sum = sum_at_owner(
        (
            jnp.dot(attn_a, out_a, preferred_element_type=jnp.float32)
            + jnp.dot(attn_b, out_b, preferred_element_type=jnp.float32)
        ).astype(jnp.bfloat16),
        "tp",
        0,
    )
    own_resid = lax.dynamic_slice_in_dim(residual, own_start, own_rows, 0)
    mixed_rows = own_resid.astype(jnp.float32) + head_sum
    normed = gathered_copies(normalize(mixed_rows, norm_gain), "tp", 0)
    gate_act = jnp.dot(normed, gate_full, preferred_element_type=jnp.float32)
    up_act = jnp.dot(normed, up_full, preferred_element_type=jnp.float32)
    hidden = (jax.nn.silu(gate_act) * up_act).astype(jnp.bfloat16)
    branch_sum = sum_at_owner(
        jnp.dot(hidden, down_full, preferred_element_type=jnp.float32).astype(jnp.bfloat16), "tp", 0
    )
    return (mixed_rows + 0.5 * branch_sum).astype(jnp.bfloat16)


def solution(mesh):
    return jax.shard_map(
        on_device,
        mesh=mesh,
        in_specs=(
            P("sp", "tp"),
            P("sp", "tp"),
            P("sp", "tp"),
            P("sp", "tp"),
            P("sp", "tp"),
            P("sp", "tp"),
            P(),
            P(),
            P("tp", None),
            P("tp", None),
            P("sp", None),
            P(),
            P("sp", "tp"),
            P("sp", "tp"),
            P("tp", "sp"),
        ),
        out_specs=P(("sp", "tp"), None),
        check_vma=False,
    )
```

profile of v0, /device:TPU:1, one launch (start us, length us, event | category | flops | bytes accessed | tf_op | source)
XLA Modules:
  0.0 315.2 jit_solution(1627057619854827771)
XLA Ops:
  6.6 0.9 slice_bitcast_fusion.20
  7.4 0.8 fusion.64
  8.2 0.8 fusion.65
  9.1 0.8 slice_bitcast_fusion.21
  9.9 0.9 fusion.59
  10.8 0.9 fusion.60
  11.7 0.1 copy.42
  11.8 0.1 copy.43
  12.0 0.1 broadcast_multiply_fusion.1
  12.2 0.9 fusion.69
  13.1 0.1 copy.44
  13.2 0.9 copy.45
  14.1 1.3 add_convert_fusion.1
  15.3 1.6 pad_maximum_fusion.3
  17.0 1.1 copy.54
  18.0 1.1 copy.55
  19.1 1.8 pad_maximum_fusion
  20.9 0.1 copy.51
  21.2 0.1 copy.47
  21.3 0.1 copy.48
  21.4 0.1 copy.46
  21.7 0.1 multiply_multiply_fusion
  21.8 0.1 fusion.54
  22.2 0.1 fusion.57
  22.3 77.9 %all-gather.3.cloned.1.call-done = bf16[6144,384]{1,0:T(8,128)(2,1)} async-done(((bf16[192,384]{1,0:T(8,128)(2,1)}), bf16[6144,384]{1,0:T(8,128)(2,1)}) %all-gather.3.cloned.1.call-update) | async-done | bytes 4718608 | tf_op jit(solution)/shard_map/all_gather | solution.py:27
  100.2 2.9 bitcast_reduce_fusion.1
  103.1 1.4 fusion.7
  104.6 0.9 copy-done.3
  105.5 1.4 fusion.38
  106.9 0.1 copy.50
  107.0 8.0 %bitcast_reduce_fusion = (f32[4,192]{1,0:T(4,128)S(1)}, f32[6144,192,4]{0,1,2:T(8,128)}) fusion(bf16[192,4,64]{0,2,1:T(8,128)(2,1)S(1)} %bitcast.178, bf16[6144,384]{1,0:T(8,128)(2,1)S(1)} %copy-done.3), kind=kOutput, calls=%fused_computation.1 | convolution fusion | flops 613416192 | bytes 20581376 | tf_op jit(solution)/shard_map/tkgd,pkd->kgtp/dot_general | solution.py:99
  115.1 2.2 fusion.61
  117.3 9.7 %fusion.1 = f32[4,192]{1,0:T(4,128)S(1)} fusion(f32[6144,192,4]{0,1,2:T(8,128)} %get-tuple-element.40, f32[4,192]{1,0:T(4,128)S(1)} %broadcast_maximum_fusion), kind=kLoop, calls=%fused_computation.3 | loop fusion | flops 14155008 | bytes 18880512 | tf_op jit(solution)/shard_map/reduce_sum | solution.py:104
  127.0 10.7 %fusion.44 = bf16[4,192,64]{1,2,0:T(8,128)(2,1)S(1)} fusion(bf16[6144,384]{1,0:T(8,128)(2,1)} %all-gather.3.cloned.1.call-done, f32[6144,192,4]{0,1,2:T(8,128)} %get-tuple-element.40, f32[4,192]{1,0:T(4,128)S(1)} %broadcast_maximum_fusion, f32[4,192]{1,0:T(4,128)S(1)} %fusion.1), kind=kOutput, calls=%fused_computation.38 | convolution fusion | flops 618233856 | bytes 20551680 | tf_op jit(solution)/shard_map/kgtp,pkd->kgtd/dot_general | solution.py:105
  137.7 1.8 fusion.15
  139.5 9.0 %all-to-all-start = ((bf16[8,24,4096]{2,1,0:T(8,128)(2,1)}), bf16[8,24,4096]{2,1,0:T(8,128)(2,1)S(1)}, u32[]{:S(2)}, u32[]{:S(2)}) async-start(bf16[8,24,4096]{2,1,0:T(8,128)(2,1)} %bitcast.171), calls=%async_computation | async-start | bytes 3145728 | tf_op jit(solution)/shard_map/all_to_all | solution.py:39
  148.5 20.6 %all-to-all-done = bf16[8,24,4096]{2,1,0:T(8,128)(2,1)S(1)} async-done(((bf16[8,24,4096]{2,1,0:T(8,128)(2,1)}), bf16[8,24,4096]{2,1,0:T(8,128)(2,1)S(1)}, u32[]{:S(2)}, u32[]{:S(2)}) %all-to-all-start) | async-done | bytes 1572896 | tf_op jit(solution)/shard_map/all_to_all | solution.py:39
  169.1 0.2 convert_reduce_fusion.1
  169.3 1.1 multiply_reduce_fusion
  170.4 1.1 multiply_convert_fusion
  171.5 0.2 broadcast_in_dim.8
  171.7 24.7 %all_to_all.15 = bf16[8,24,4096]{2,1,0:T(8,128)(2,1)} all-to-all(bf16[8,24,4096]{2,1,0:T(8,128)(2,1)S(1)} %broadcast_in_dim.8), channel_id=1, replica_groups=mesh['sp'=32,'tp'=8] {'tp'}, dimensions={0} | all-to-all | bytes 3145728 | tf_op jit(solution)/shard_map/all_to_all | solution.py:45
  196.3 65.0 %all-gather.5.cloned.1.call-done = bf16[4096,2304]{0,1:T(8,128)(2,1)} async-done(((bf16[128,2304]{0,1:T(8,128)(2,1)}), bf16[4096,2304]{0,1:T(8,128)(2,1)}) %all-gather.5.cloned.1.call-update) | async-done | bytes 18874384 | tf_op jit(solution)/shard_map/all_gather | solution.py:16
  261.3 5.5 %fusion.13 = f32[192,768]{1,0:T(8,128)S(1)} fusion(bf16[192,4096]{1,0:T(8,128)(2,1)} %bitcast.174, bf16[4096,2304]{0,1:T(8,128)(2,1)} %all-gather.5.cloned.1.call-done), kind=kOutput, calls=%fused_computation.17 | convolution fusion | flops 1207959552 | bytes 8454144 | tf_op jit(solution)/shard_map/dot_general | solution.py:180
  266.8 10.9 %fusion.16 = bf16[192,4096]{1,0:T(8,128)(2,1)} fusion(bf16[4096,2304]{0,1:T(8,128)(2,1)} %all-gather.5.cloned.1.call-done, bf16[192,4096]{1,0:T(8,128)(2,1)} %bitcast.175, f32[192,768]{1,0:T(8,128)S(1)} %fusion.13), kind=kOutput, calls=%fused_computation.21 | convolution fusion | flops 2417590272 | bytes 16318464 | tf_op jit(solution)/shard_map/dot_general | solution.py:184
  277.7 28.8 %all_to_all.16 = bf16[8,24,4096]{2,1,0:T(8,128)(2,1)S(1)} all-to-all(bf16[8,24,4096]{2,1,0:T(8,128)(2,1)} %bitcast.176), channel_id=1, replica_groups=mesh['sp'=32,'tp'=8] {'tp'}, dimensions={0} | all-to-all | bytes 3145728 | tf_op jit(solution)/shard_map/all_to_all | solution.py:39
  306.5 0.2 convert_reduce_fusion
  306.7 1.7 add_convert_fusion
  (46 shorter events, 0.8 us)
Async XLA Ops:
  6.5 108.5 %copy-start = (bf16[256,4096]{1,0:T(8,128)(2,1)S(1)}, bf16[256,4096]{1,0:T(8,128)(2,1)}, u32[]{:S(2)}) copy-start(bf16[256,4096]{1,0:T(8,128)(2,1)} %param.23) | copy-start | bytes 6291460
  6.5 14.4 %copy-start.5 = (bf16[192,256]{1,0:T(8,128)(2,1)S(1)}, bf16[192,256]{1,0:T(8,128)(2,1)}, u32[]{:S(2)}) copy-start(bf16[192,256]{1,0:T(8,128)(2,1)} %param.18) | copy-start | bytes 294916
  6.5 14.9 %copy-start.6 = (bf16[192,256]{1,0:T(8,128)(2,1)S(1)}, bf16[192,256]{1,0:T(8,128)(2,1)}, u32[]{:S(2)}) copy-start(bf16[192,256]{1,0:T(8,128)(2,1)} %param.15) | copy-start | bytes 294916
  6.5 93.6 %all-gather.3.cloned.1.call-start = ((), (), s32[]{:S(2)}) async-start(), calls=%async_computation.3 | async-start | bytes 4866048 | tf_op jit(solution)/shard_map/all_gather | solution.py:27
  16.9 244.4 %all-gather.5.cloned.1.call-start = ((), (), s32[]{:S(2)}) async-start(), calls=%async_computation.4 | async-start | bytes 19464192 | tf_op jit(solution)/shard_map/all_gather | solution.py:16
  103.1 2.3 copy-start.3
  127.0 10.7 %copy-start.2 = (f32[192,4096]{1,0:T(8,128)S(1)}, f32[192,4096]{1,0:T(8,128)}, u32[]{:S(2)}) copy-start(f32[192,4096]{1,0:T(8,128)} %fusion.61) | copy-start | bytes 9437188
  127.0 10.7 %copy-start.4 = (bf16[256,4096]{1,0:T(8,128)(2,1)S(1)}, bf16[256,4096]{1,0:T(8,128)(2,1)}, u32[]{:S(2)}) copy-start(bf16[256,4096]{1,0:T(8,128)(2,1)} %param.24) | copy-start | bytes 6291460
  137.7 32.7 %copy-start.7 = (f32[4096]{0:T(1024)S(1)}, f32[4096]{0:T(1024)}, u32[]{:S(2)}) copy-start(f32[4096]{0:T(1024)} %param.26) | copy-start | bytes 49156
  139.5 29.6 %all-to-all-start = ((bf16[8,24,4096]{2,1,0:T(8,128)(2,1)}), bf16[8,24,4096]{2,1,0:T(8,128)(2,1)S(1)}, u32[]{:S(2)}, u32[]{:S(2)}) async-start(bf16[8,24,4096]{2,1,0:T(8,128)(2,1)} %bitcast.171), calls=%async_computation | async-start | bytes 3145728 | tf_op jit(solution)/shard_map/all_to_all | solution.py:39
  266.8 41.6 %copy-start.1 = (bf16[256,4096]{1,0:T(8,128)(2,1)S(1)}, bf16[256,4096]{1,0:T(8,128)(2,1)}, u32[]{:S(2)}) copy-start(bf16[256,4096]{1,0:T(8,128)(2,1)} %param.23) | copy-start | bytes 6291460
Sparse Core Ops, SparseCore 0:
  17.0 83.1 all-gather.2
  102.6 158.6 all-gather.4
where the time goes:
time: 316 us; the launch traced here: 315 us
  waiting for transfers between devices  163 us (52%)
  blocking collectives  53.4 us (17%)
  matrix products  43.4 us (14%)
  other arithmetic  25.2 us (8%)
  between operations  13.8 us (4%)
  starting transfers between devices  9.09 us (3%)
  local copies, waits for them, and re-layouts  6.82 us (2%)
    all_gather x1, waiting for transfers between devices, side_by_side(): filled = lax.all_gather(both, axis, axis=dim, tiled=True)  77.9 us
    all_gather x1, waiting for transfers between devices, rows_first(): filled, at, outs = (lax.all_gather(both, axis, axis=0, tiled=True), 0, [])  65 us
    all_to_all x1, blocking collectives, sum_at_owner(): lax.all_to_all(parts, axis, split_axis=0, concat_axis=0, tiled=True)  28.8 us
    all_to_all x1, blocking collectives, copy_for_each(): lax.all_to_all(jnp.broadcast_to(value[None], (devices, *value.shape)), ax...  24.7 us
    all_to_all x1, waiting for transfers between devices, sum_at_owner(): lax.all_to_all(parts, axis, split_axis=0, concat_axis=0, tiled=True)  20.6 us
    dot_general x2, matrix products, attend(): jnp.einsum('kgtp,pkd->kgtd', exp_scores.astype(jnp.bfloat16), v_heads, pr...  12.1 us
    reduce_sum x2, other arithmetic, attend(): new_sum = jnp.sum(exp_scores, axis=-1)  11.1 us
    dot_general x2, matrix products, attend(): jnp.einsum('tkgd,pkd->kgtp', q_heads, k_heads, preferred_element_type=jnp...  11 us
  transfers between devices with their start and end apart: 3, of which 3 were waited for; matrix products, arithmetic and copies ran while one was open for 15% of the time, Pallas kernels for 0%

commit v1 on v0

--- a/solution.py
+++ b/solution.py
@@ -13,7 +13,13 @@
 def rows_first(arrays, axis, dims):
     turned = [jnp.moveaxis(a, dim, 0) for a, dim in zip(arrays, dims)]
     both = jnp.concatenate([t.reshape(len(t), -1) for t in turned], axis=1)
-    filled, at, outs = (lax.all_gather(both, axis, axis=0, tiled=True), 0, [])
+    filled, at, outs = (
+        jnp.concatenate(
+            lax.all_to_all(jnp.stack([both] * lax.axis_size(axis)), axis, 0, 0), axis=0
+        ),
+        0,
+        [],
+    )
     for t, dim in zip(turned, dims):
         share = filled[:, at : at + t[0].size].reshape(-1, *t.shape[1:])
         outs.append(jnp.moveaxis(share, 0, dim))

time: 316 us -> 667 us (2.11)
  blocking collectives: 53.4 us -> 440 us
  waiting for transfers between devices: 163 us -> 121 us
  local copies, waits for them, and re-layouts: 6.82 us -> 15.9 us
    all_to_all x1, blocking collectives: 24.7 us -> 413 us  [rows_first(): lax.all_to_all(jnp.stack([both] * lax.axis_size(axis)), axis, 0, 0)]
    all_gather x1 -> x0, waiting for transfers between devices: 65 us -> none  [rows_first(): filled, at, outs = (lax.all_gather(both, axis, axis=0, tiled=True), 0, [])]
    all_to_all x0 -> x1, waiting for transfers between devices: none -> 20.1 us  [copy_for_each(): lax.all_to_all(jnp.broadcast_to(value[None], (devices, *value.shape)), ax...]
  transfers between devices with their start and end apart: 3 -> 3, of which waited for: 3 -> 3; matrix products, arithmetic and copies ran while one was open for 15% -> 1% of each run, Pallas kernels for 0% -> 0%
where the time goes in v1:
time: 667 us; the launch traced here: 666 us
  blocking collectives  440 us (66%)
  waiting for transfers between devices  121 us (18%)
  matrix products  38.6 us (6%)
  other arithmetic  23.3 us (3%)
  local copies, waits for them, and re-layouts  15.9 us (2%)
  starting transfers between devices  13.8 us (2%)
  between operations  13.7 us (2%)
    all_to_all x1, blocking collectives, rows_first(): lax.all_to_all(jnp.stack([both] * lax.axis_size(axis)), axis, 0, 0)  413 us
    all_gather x1, waiting for transfers between devices, side_by_side(): filled = lax.all_gather(both, axis, axis=dim, tiled=True)  80.1 us
    all_to_all x1, blocking collectives, sum_at_owner(): lax.all_to_all(parts, axis, split_axis=0, concat_axis=0, tiled=True)  27 us
    all_to_all x1, waiting for transfers between devices, sum_at_owner(): lax.all_to_all(parts, axis, split_axis=0, concat_axis=0, tiled=True)  20.6 us
    all_to_all x1, waiting for transfers between devices, copy_for_each(): lax.all_to_all(jnp.broadcast_to(value[None], (devices, *value.shape)), ax...  20.1 us
  transfers between devices with their start and end apart: 3, of which 3 were waited for; matrix products, arithmetic and copies ran while one was open for 1% of the time, Pallas kernels for 0%

profile of v1, /device:TPU:1, one launch (start us, length us, event | category | flops | bytes accessed | tf_op | source)
XLA Modules:
  0.0 666.4 jit_solution(18058287617744468619)
XLA Ops:
  6.6 0.9 slice_bitcast_fusion.20
  7.4 0.8 fusion.64
  8.2 0.8 fusion.65
  9.1 0.8 slice_bitcast_fusion.21
  9.9 0.9 fusion.59
  10.8 0.9 fusion.60
  11.7 0.1 copy.44
  12.0 0.1 broadcast_multiply_fusion.1
  12.1 0.9 fusion.69
  13.0 0.1 copy.46
  13.2 0.9 copy.47
  14.0 1.3 add_convert_fusion.1
  15.3 1.6 pad_maximum_fusion.3
  16.9 1.0 copy.53
  18.1 0.1 copy.49
  18.2 0.1 copy.50
  18.3 1.0 copy.48
  19.6 0.1 fusion.54
  19.9 0.1 fusion.57
  20.0 80.1 %all-gather.2.cloned.1.call-done = bf16[6144,384]{1,0:T(8,128)(2,1)} async-done(((bf16[192,384]{1,0:T(8,128)(2,1)}), bf16[6144,384]{1,0:T(8,128)(2,1)}) %all-gather.2.cloned.1.call-update) | async-done | bytes 4718608 | tf_op jit(solution)/shard_map/all_gather | solution.py:33
  100.2 9.5 %bitcast_reduce_fusion = (f32[4,192]{1,0:T(4,128)S(1)}, f32[6144,192,4]{0,1,2:T(8,128)}) fusion(bf16[192,4,64]{0,2,1:T(8,128)(2,1)S(1)} %bitcast.179, bf16[6144,384]{1,0:T(8,128)(2,1)} %all-gather.2.cloned.1.call-done), kind=kOutput, calls=%fused_computation.1 | convolution fusion | flops 613416192 | bytes 20548608 | tf_op jit(solution)/shard_map/tkgd,pkd->kgtp/dot_general | solution.py:105
  109.6 1.5 bitcast_reduce_fusion.1
  111.2 1.4 fusion.7
  112.6 1.4 fusion.38
  114.1 0.1 copy.52
  114.2 9.5 %fusion.1 = f32[4,192]{1,0:T(4,128)S(1)} fusion(f32[6144,192,4]{0,1,2:T(8,128)} %get-tuple-element.40, f32[4,192]{1,0:T(4,128)S(1)} %broadcast_maximum_fusion), kind=kLoop, calls=%fused_computation.3 | loop fusion | flops 14155008 | bytes 18880512 | tf_op jit(solution)/shard_map/reduce_sum | solution.py:110
  123.7 0.6 fusion.61
  124.3 10.5 %fusion.44 = bf16[4,192,64]{1,2,0:T(8,128)(2,1)S(1)} fusion(bf16[6144,384]{1,0:T(8,128)(2,1)} %all-gather.2.cloned.1.call-done, f32[6144,192,4]{0,1,2:T(8,128)} %get-tuple-element.40, f32[4,192]{1,0:T(4,128)S(1)} %broadcast_maximum_fusion, f32[4,192]{1,0:T(4,128)S(1)} %fusion.1), kind=kOutput, calls=%fused_computation.38 | convolution fusion | flops 618233856 | bytes 20551680 | tf_op jit(solution)/shard_map/kgtp,pkd->kgtd/dot_general | solution.py:111
  134.8 2.0 fusion.15
  136.9 8.6 %all-to-all-start = ((bf16[8,24,4096]{2,1,0:T(8,128)(2,1)}), bf16[8,24,4096]{2,1,0:T(8,128)(2,1)S(1)}, u32[]{:S(2)}, u32[]{:S(2)}) async-start(bf16[8,24,4096]{2,1,0:T(8,128)(2,1)} %bitcast.174), calls=%async_computation | async-start | bytes 3145728 | tf_op jit(solution)/shard_map/all_to_all | solution.py:45
  145.5 20.6 %all-to-all-done = bf16[8,24,4096]{2,1,0:T(8,128)(2,1)S(1)} async-done(((bf16[8,24,4096]{2,1,0:T(8,128)(2,1)}), bf16[8,24,4096]{2,1,0:T(8,128)(2,1)S(1)}, u32[]{:S(2)}, u32[]{:S(2)}) %all-to-all-start) | async-done | bytes 1572896 | tf_op jit(solution)/shard_map/all_to_all | solution.py:45
  166.1 0.2 convert_reduce_fusion.1
  166.3 1.1 multiply_reduce_fusion
  167.4 1.0 multiply_convert_fusion
  168.4 1.3 broadcast_in_dim.8
  169.8 5.1 all-to-all-start.1
  174.9 0.2 copy.56
  175.1 0.2 copy.57
  175.3 0.2 copy.58
  175.6 20.1 %all-to-all-done.1 = bf16[8,24,4096]{2,1,0:T(8,128)(2,1)} async-done(((bf16[8,24,4096]{2,1,0:T(8,128)(2,1)}), bf16[8,24,4096]{2,1,0:T(8,128)(2,1)}, u32[]{:S(2)}, u32[]{:S(2)}) %all-to-all-start.1) | async-done | bytes 1572896 | tf_op jit(solution)/shard_map/all_to_all | solution.py:51
  195.6 2.2 stack.14
  197.8 413.3 %all_to_all.20 = bf16[32,128,2304]{2,1,0:T(8,128)(2,1)S(1)} all-to-all(bf16[32,128,2304]{2,1,0:T(8,128)(2,1)S(1)} %stack.14), channel_id=1, replica_groups=mesh['sp'=32,'tp'=8] {'sp'}, dimensions={0} | all-to-all | bytes 37748736 | tf_op jit(solution)/shard_map/all_to_all | solution.py:18
  611.1 6.5 copy-done.2
  617.5 2.8 fusion.13
  620.4 10.2 %fusion.16 = bf16[192,4096]{1,0:T(8,128)(2,1)} fusion(bf16[4096,2304]{1,0:T(8,128)(2,1)} %bitcast.173, bf16[192,4096]{1,0:T(8,128)(2,1)} %bitcast.41, f32[192,768]{1,0:T(8,128)S(1)} %fusion.13), kind=kOutput, calls=%fused_computation.21 | convolution fusion | flops 2417590272 | bytes 16318464 | tf_op jit(solution)/shard_map/dot_general | solution.py:190
  630.6 27.0 %all_to_all.21 = bf16[8,24,4096]{2,1,0:T(8,128)(2,1)S(1)} all-to-all(bf16[8,24,4096]{2,1,0:T(8,128)(2,1)} %bitcast.177), channel_id=1, replica_groups=mesh['sp'=32,'tp'=8] {'tp'}, dimensions={0} | all-to-all | bytes 3145728 | tf_op jit(solution)/shard_map/all_to_all | solution.py:45
  657.6 0.2 convert_reduce_fusion
  657.8 1.7 add_convert_fusion
  (49 shorter events, 1.0 us)
Async XLA Ops:
  6.5 117.2 %copy-start = (bf16[256,4096]{1,0:T(8,128)(2,1)S(1)}, bf16[256,4096]{1,0:T(8,128)(2,1)}, u32[]{:S(2)}) copy-start(bf16[256,4096]{1,0:T(8,128)(2,1)} %param.23) | copy-start | bytes 6291460
  6.5 93.6 %all-gather.2.cloned.1.call-start = ((), (), s32[]{:S(2)}) async-start(), calls=%async_computation.4 | async-start | bytes 4866048 | tf_op jit(solution)/shard_map/all_gather | solution.py:33
  100.2 9.5 %copy-start.3 = (bf16[6144,384]{1,0:T(8,128)(2,1)S(1)}, bf16[6144,384]{1,0:T(8,128)(2,1)}, u32[]{:S(2)}) copy-start(bf16[6144,384]{1,0:T(8,128)(2,1)} %all-gather.2.cloned.1.call-done) | copy-start | bytes 14155780
  124.3 10.5 %copy-start.4 = (bf16[256,4096]{1,0:T(8,128)(2,1)S(1)}, bf16[256,4096]{1,0:T(8,128)(2,1)}, u32[]{:S(2)}) copy-start(bf16[256,4096]{1,0:T(8,128)(2,1)} %param.24) | copy-start | bytes 6291460
  134.8 32.6 %copy-start.8 = (f32[4096]{0:T(1024)S(1)}, f32[4096]{0:T(1024)}, u32[]{:S(2)}) copy-start(f32[4096]{0:T(1024)} %param.26) | copy-start | bytes 49156
  136.9 29.2 %all-to-all-start = ((bf16[8,24,4096]{2,1,0:T(8,128)(2,1)}), bf16[8,24,4096]{2,1,0:T(8,128)(2,1)S(1)}, u32[]{:S(2)}, u32[]{:S(2)}) async-start(bf16[8,24,4096]{2,1,0:T(8,128)(2,1)} %bitcast.174), calls=%async_computation | async-start | bytes 3145728 | tf_op jit(solution)/shard_map/all_to_all | solution.py:45
  145.5 29.4 %copy-start.6 = (bf16[128,768]{1,0:T(8,128)(2,1)S(1)}, bf16[128,768]{1,0:T(8,128)(2,1)}, u32[]{:S(2)}) copy-start(bf16[128,768]{1,0:T(8,128)(2,1)} %param.27) | copy-start | bytes 589828
  145.5 29.6 %copy-start.7 = (bf16[128,768]{1,0:T(8,128)(2,1)S(1)}, bf16[128,768]{1,0:T(8,128)(2,1)}, u32[]{:S(2)}) copy-start(bf16[128,768]{1,0:T(8,128)(2,1)} %param.28) | copy-start | bytes 589828
  145.5 29.8 %copy-start.5 = (bf16[768,128]{1,0:T(8,128)(2,1)S(1)}, bf16[768,128]{1,0:T(8,128)(2,1)}, u32[]{:S(2)}) copy-start(bf16[768,128]{1,0:T(8,128)(2,1)} %param.29) | copy-start | bytes 589828
  169.8 25.9 %all-to-all-start.1 = ((bf16[8,24,4096]{2,1,0:T(8,128)(2,1)}), bf16[8,24,4096]{2,1,0:T(8,128)(2,1)}, u32[]{:S(2)}, u32[]{:S(2)}) async-start(bf16[8,24,4096]{2,1,0:T(8,128)(2,1)} %broadcast_in_dim.8), calls=%async_computation.1 | async-start | bytes 3145728 | tf_op jit(solution)/shard_map/all_to_all | solution.py:51
  611.1 6.5 copy-start.2
  620.4 39.1 %copy-start.1 = (bf16[256,4096]{1,0:T(8,128)(2,1)S(1)}, bf16[256,4096]{1,0:T(8,128)(2,1)}, u32[]{:S(2)}) copy-start(bf16[256,4096]{1,0:T(8,128)(2,1)} %param.23) | copy-start | bytes 6291460
Sparse Core Ops, SparseCore 0:
  17.0 83.1 all-gather.1
